TPU v7x, 32 devices: a whole 2x2x4 slice. The times are simulated.
32 devices in a mesh: sp: 8 (over z, y), tp: 4 (over x, core).
Axes of the slice: x: 2, y: 2, z: 4, core: 2. Of those that a mesh axis runs over, the one named last changes fastest.
Arguments:
- residual: bfloat16 [5120, 2048], P(('sp', 'tp')), may hold values from -6 to 6
- small_value_inputs: bfloat16 [5120, 1024], P('sp', 'tp'), may hold values from -6 to 6
- large_value_inputs: bfloat16 [5120, 1024], P('sp', 'tp'), may hold values from -6 to 6
- small_gate_inputs: bfloat16 [5120, 1024], P('sp', 'tp'), may hold values from -6 to 6
- large_gate_inputs: bfloat16 [5120, 1024], P('sp', 'tp'), may hold values from -6 to 6
- state_projections: bfloat16 [5120, 4, 128], P('sp'), may hold values from -6 to 6
- small_step_inputs: bfloat16 [5120, 16], P('sp', 'tp'), may hold values from -2.5 to 2.5
- large_step_inputs: bfloat16 [5120, 8], P('sp', 'tp'), may hold values from -2.5 to 2.5
- small_decay_offsets: float32 [5120, 16], P('sp', 'tp'), may hold values from -1.4 to 0
- large_decay_offsets: float32 [5120, 8], P('sp', 'tp'), may hold values from -1.4 to 0
- small_decay_rates: float32 [16], P('tp'), may hold values from -11.1 to -3.1
- large_decay_rates: float32 [8], P('tp'), may hold values from -11.1 to -3.1
- small_filter_taps: bfloat16 [4, 1024], P(None, 'tp'), may hold values from -3 to 3
- large_filter_taps: bfloat16 [4, 1024], P(None, 'tp'), may hold values from -3 to 3
- state_filter_taps: bfloat16 [4, 4, 128], replicated, may hold values from -3 to 3
- small_head_gains: float32 [1024], P('tp'), may hold values from 0.1 to 1.9
- large_head_gains: float32 [1024], P('tp'), may hold values from 0.1 to 1.9
- small_output_projection: bfloat16 [1024, 2048], P('tp'), may hold values from -0.125 to 0.125
- large_output_projection: bfloat16 [1024, 2048], P('tp'), may hold values from -0.125 to 0.125
- channel_norm_gain: float32 [2048], replicated, may hold values from 0.1 to 1.9
- gate_matrix: bfloat16 [2048, 5632], P('sp', 'tp'), may hold values from -0.125 to 0.125
- up_matrix: bfloat16 [2048, 5632], P('sp', 'tp'), may hold values from -0.125 to 0.125
- down_matrix: bfloat16 [5632, 2048], P('tp', 'sp'), may hold values from -0.078125 to 0.078125
Outputs:
- layer_out: bfloat16 [5120, 2048], P(('sp', 'tp'))
All inputs are finite; a program needn't handle non-finite values.
Results may differ from a plain program's by a relative error of at most 0.015.
Values may be sent and summed in bfloat16 or wider, within the bound.
A program may use at most 64 MiB of HBM per device.

v0:
```python
import jax
import jax.numpy as jnp
from jax import lax
from jax.experimental import pallas as pl
from jax.experimental.pallas import tpu as pltpu
from jax.sharding import PartitionSpec as P


HIGH = lax.Precision.HIGHEST
head_eps = 1e-05
row_eps = 1e-06
BF = jnp.bfloat16
F32 = jnp.float32
MESH = pl.DeviceIdType.MESH
LANE = 128


def ring_order(n):
    ys = 1
    while ys * ys * 4 <= n:
        ys *= 2
    zs = n // ys
    if ys * zs != n or ys < 2 or zs % 2:
        return list(range(n))
    walk = []
    for z in range(zs):
        row = list(range(1, ys))
        walk += [z * ys + y for y in (row if z % 2 == 0 else row[::-1])]
    return walk + [z * ys for z in reversed(range(zs))]


def causal_conv(series, prior, taps):
    width, length = taps.shape[0], series.shape[0]
    padded = jnp.concatenate([prior, series], axis=0).astype(F32)
    total = jnp.zeros(series.shape, F32)
    for offset in range(width):
        total = total + taps[offset].astype(F32)[None, :] * padded[offset : offset + length]
    return jax.nn.silu(total)


def local_heads(conv_values, step, within, keys, reads):
    length, width = conv_values.shape
    heads = step.shape[1]
    size = width // heads
    driven = conv_values.reshape(length, heads, size) * step[:, :, None]
    scores = lax.dot_general(reads, keys, (((1,), (1,)), ((), ())), preferred_element_type=F32)
    mask = jnp.tril(jnp.ones((length, length), dtype=bool))
    outs, finals = [], []
    for h in range(heads):
        own = within[:, h]
        spread = jnp.where(mask, own[:, None] - own[None, :], 0.0)
        mixing = jnp.where(mask, jnp.exp(spread) * scores, 0.0).astype(BF)
        value = driven[:, h]
        outs.append(jnp.dot(mixing, value.astype(BF), preferred_element_type=F32))
        late = (value * jnp.exp(own[-1] - own)[:, None]).astype(BF)
        finals.append(
            lax.dot_general(late, keys, (((0,), (0,)), ((), ())), preferred_element_type=F32)
        )
    return outs, jnp.concatenate(finals, axis=0)


def finish_heads(outs, incoming, within, reads, gate_inputs, gains):
    size = outs[0].shape[1]
    done = []
    carried = lax.dot_general(
        reads, incoming.astype(BF), (((1,), (1,)), ((), ())), preferred_element_type=F32
    )
    for h, local in enumerate(outs):
        cols = slice(h * size, (h + 1) * size)
        scan_out = local + carried[:, cols] * jnp.exp(within[:, h])[:, None]
        gated = scan_out * jax.nn.silu(gate_inputs[:, cols].astype(F32))
        scale = lax.rsqrt(jnp.mean(gated * gated, axis=-1, keepdims=True) + head_eps)
        done.append((gated * scale * gains[cols][None, :]).astype(BF))
    return jnp.concatenate(done, axis=1)


def row_norm(rows, gain):
    wide = rows.astype(F32)
    scale = lax.rsqrt(jnp.mean(wide * wide, axis=-1, keepdims=True) + row_eps)
    return (wide * scale * gain[None, :]).astype(BF)


def ring_gather(own):
    n = lax.axis_size("sp")
    order = ring_order(n)
    place = [order.index(i) for i in range(n)]
    me = lax.axis_index("sp")
    at = jnp.asarray(place, jnp.int32)[me]
    owners = jnp.asarray(order, jnp.int32)
    ahead = [(order[i], order[(i + 1) % n]) for i in range(n)]
    back = [(b, a) for a, b in ahead]
    rows = own.shape[0]
    whole = jnp.zeros((n * rows,) + own.shape[1:], own.dtype)
    whole = lax.dynamic_update_slice(whole, own, (me * rows, 0))
    up = down = own
    half = n // 2
    for k in range(1, half + 1):
        from_up = owners[(at - k) % n] * rows
        from_down = owners[(at + k) % n] * rows
        if 2 * k == n:
            cut = rows // 2
            up, down = up[:cut], down[cut:]
            from_down = from_down + cut
        up = lax.ppermute(up, "sp", ahead)
        down = lax.ppermute(down, "sp", back)
        whole = lax.dynamic_update_slice(whole, up, (from_up, 0))
        whole = lax.dynamic_update_slice(whole, down, (from_down, 0))
    return whole


def on_device(
    residual,
    small_value_inputs,
    large_value_inputs,
    small_gate_inputs,
    large_gate_inputs,
    state_projections,
    small_step_inputs,
    large_step_inputs,
    small_decay_offsets,
    large_decay_offsets,
    small_decay_rates,
    large_decay_rates,
    small_filter_taps,
    large_filter_taps,
    state_filter_taps,
    small_head_gains,
    large_head_gains,
    small_output_projection,
    large_output_projection,
    channel_norm_gain,
    gate_matrix,
    up_matrix,
    down_matrix,
):
    n = lax.axis_size("sp")
    me = lax.axis_index("sp")
    margin = state_filter_taps.shape[0] - 1
    length, w1 = small_value_inputs.shape
    w2 = large_value_inputs.shape[1]
    state = state_projections.shape[2]
    planes = state_projections.shape[1] * state
    units = gate_matrix.shape[1]
    flat = state_projections.reshape(length, planes)
    series = jnp.concatenate([small_value_inputs, large_value_inputs, flat], axis=1)
    prior = lax.ppermute(
        series[length - margin :], "sp", [(i, i + 1) for i in range(n - 1)]
    )
    pack = jnp.concatenate([gate_matrix, up_matrix, down_matrix.T], axis=1)
    pack, prior = lax.optimization_barrier((pack, prior))
    whole = ring_gather(pack)

    taps = jnp.concatenate(
        [small_filter_taps, large_filter_taps, state_filter_taps.reshape(margin + 1, planes)], axis=1
    )
    conv = causal_conv(series, prior, taps)
    maps = conv[:, w1 + w2 :].astype(BF)
    keys1, reads1, keys2, reads2 = (maps[:, i * state : (i + 1) * state] for i in range(4))

    heads1 = small_decay_rates.shape[0]
    step = jax.nn.softplus(
        jnp.concatenate([small_step_inputs, large_step_inputs], axis=1).astype(F32)
    )
    rates = jnp.concatenate([small_decay_rates, large_decay_rates])
    offsets = jnp.concatenate([small_decay_offsets, large_decay_offsets], axis=1)
    log_decay = -jnp.exp(rates)[None, :] * step + offsets
    lower = jnp.tril(jnp.ones((length, length), F32))
    within = jnp.dot(lower, log_decay, precision=HIGH)

    outs1, final1 = local_heads(conv[:, :w1], step[:, :heads1], within[:, :heads1], keys1, reads1)
    outs2, final2 = local_heads(
        conv[:, w1 : w1 + w2], step[:, heads1:], within[:, heads1:], keys2, reads2
    )
    heads = rates.shape[0]
    total = jnp.exp(within[-1])
    row = jnp.pad(total[None, :], ((0, 15), (0, state - heads)))
    sent = jnp.concatenate([final1, final2, row], axis=0).astype(BF)
    gathered = lax.all_gather(sent, "sp").astype(F32)
    states1 = gathered[:, :w1].reshape(n, heads1, w1 // heads1, state)
    states2 = gathered[:, w1 : w1 + w2].reshape(n, heads - heads1, w2 // (heads - heads1), state)
    totals = gathered[:, w1 + w2, :heads]
    carry1, carry2 = jnp.zeros_like(states1[0]), jnp.zeros_like(states2[0])
    for hop in range(n - 1):
        factor1 = totals[hop, :heads1][:, None, None]
        factor2 = totals[hop, heads1:][:, None, None]
        carry1 = jnp.where(hop < me, carry1 * factor1 + states1[hop], carry1)
        carry2 = jnp.where(hop < me, carry2 * factor2 + states2[hop], carry2)
    carry1, carry2 = carry1.reshape(w1, state), carry2.reshape(w2, state)

    heads_small = finish_heads(
        outs1, carry1, within[:, :heads1], reads1, small_gate_inputs, small_head_gains
    )
    heads_large = finish_heads(
        outs2, carry2, within[:, heads1:], reads2, large_gate_inputs, large_head_gains
    )
    mixed = (
        jnp.dot(heads_small, small_output_projection, preferred_element_type=F32)
        + jnp.dot(heads_large, large_output_projection, preferred_element_type=F32)
    ).astype(BF)
    mixed = lax.psum_scatter(
        mixed,
        "tp",
        scatter_dimension=0,
        tiled=True,
    ).astype(F32)
    middle = (residual.astype(F32) + mixed).astype(BF)
    normed = row_norm(middle, channel_norm_gain)
    normed_all = lax.all_gather(normed, "tp", axis=0, tiled=True)
    gate = jnp.dot(normed_all, whole[:, :units], preferred_element_type=F32)
    up = jnp.dot(normed_all, whole[:, units : 2 * units], preferred_element_type=F32)
    hidden = (jax.nn.silu(gate) * up).astype(BF)
    partial = lax.dot_general(
        hidden, whole[:, 2 * units :], (((1,), (1,)), ((), ())), preferred_element_type=F32
    )
    down = lax.psum_scatter(
        partial.astype(BF), "tp", scatter_dimension=0, tiled=True
    ).astype(F32)
    return (middle.astype(F32) + down).astype(BF)


def geometry(n):
    ys = 1
    while ys * ys * 4 <= n:
        ys *= 2
    return ys, n // ys


def paired(n, tp, units):
    ys, zs = geometry(n)
    return ys == 2 and zs == 4 and tp == 4 and units % LANE == 0


def fused_kernel(
    vs,
    vl,
    gs,
    gl,
    flat,
    steps_s,
    steps_l,
    offs_s,
    offs_l,
    rates_s,
    rates_l,
    taps_s,
    taps_l,
    taps_m,
    gain_s,
    gain_l,
    proj_s,
    proj_l,
    resid,
    cgain,
    gate_m,
    up_m,
    down_m,
    out,
    xbuf,
    gbuf,
    pbuf,
    rbuf,
    hrow,
    srow,
    wrow,
    wcol,
    maps,
    drv,
    late,
    run,
    smsg,
    rmsg,
    loc,
    hbuf,
    part,
    d2d,
    xsend,
    xrecv,
    mid,
    nall,
    hid,
    wg,
    wu,
    wd,
    psum,
    dcol,
    s1,
    k1,
    r1,
    s2,
    k2,
    r2,
    lsem,
    hs_sem,
    hr_sem,
    ws_sem,
    wy_sem,
    wr_sem,
    wl_sem,
    ms_sem,
    mr_sem,
    ds_sem,
    dr_sem,
    xs_sem,
    xr_sem,
    as_sem,
    ar_sem,
    p_sem,
    q_sem,
    f1s_sem,
    f1r_sem,
    f2s_sem,
    f2r_sem,
):
    n = lax.axis_size("sp")
    sp, tp = lax.axis_index("sp"), lax.axis_index("tp")
    z, y = sp // 2, sp % 2
    pair, zz = z // 2, z % 2
    x, c = tp // 2, tp % 2
    length, w1 = vs.shape
    w2 = vl.shape[1]
    width = w1 + w2
    planes = flat.shape[1]
    state = planes // 4
    heads1, heads2 = steps_s.shape[0], steps_l.shape[0]
    halo = xbuf.shape[0] - length
    rows, units = gate_m.shape
    cols = down_m.shape[1]
    half = wg.shape[1]
    lift = units - half
    own = resid.shape[0]
    tokens = nall.shape[0]
    model = nall.shape[1]
    inner = jnp.where(pair != zz, 1, 0) == 1
    dz = 1 - 2 * pair

    def at(zi, yi):
        return (zi * 2 + yi, tp)

    mate_z = at(z + 1 - 2 * zz, y)
    mate_y = at(z, 1 - y)
    mate_x = (sp, (1 - x) * 2 + c)
    mate_c = (sp, x * 2 + 1 - c)

    def remote(src, dst, send, recv, device):
        return pltpu.make_async_remote_copy(
            src_ref=src, dst_ref=dst, send_sem=send, recv_sem=recv, device_id=device, device_id_type=MESH
        )

    barrier = pltpu.get_barrier_semaphore()
    peers = [(lax.rem(sp + k, n), tp) for k in range(1, n)] + [mate_x, mate_c]
    for peer in peers:
        pl.semaphore_signal(barrier, inc=1, device_id=peer, device_id_type=MESH)
    loads = []
    for src, dst in (
        (vs, xbuf.at[pl.ds(halo, length), pl.ds(0, w1)]),
        (vl, xbuf.at[pl.ds(halo, length), pl.ds(w1, w2)]),
        (flat, xbuf.at[pl.ds(halo, length), pl.ds(width, planes)]),
        (gs, gbuf.at[:, pl.ds(0, w1)]),
        (gl, gbuf.at[:, pl.ds(w1, w2)]),
        (proj_s, pbuf.at[pl.ds(0, w1), :]),
        (proj_l, pbuf.at[pl.ds(w1, w2), :]),
        (resid, rbuf),
    ):
        copy = pltpu.make_async_copy(src, dst, lsem.at[len(loads)])
        copy.start()
        loads.append(copy)
    pl.semaphore_wait(barrier, len(peers))

    halos = []
    for i, (src, lo, size) in enumerate(((vs, 0, w1), (vl, w1, w2), (flat, width, planes))):
        halos.append(
            remote(
                src.at[pl.ds(length - halo, halo), :],
                xbuf.at[pl.ds(0, halo), pl.ds(lo, size)],
                hs_sem.at[i],
                hr_sem.at[i],
                (lax.rem(sp + 1, n), tp),
            )
        )

    @pl.when(sp < n - 1)
    def _():
        for copy in halos:
            copy.start()

    def source(p, h):
        cut = pl.ds(pl.multiple_of(h * lift, LANE), half)
        return (gate_m.at[:, cut], up_m.at[:, cut], down_m.at[cut, :])[p]

    def place(p, b):
        if p == 2:
            return wd.at[b]
        return (wg, wu)[p].at[pl.ds(pl.multiple_of(b * rows, rows), rows), :]

    def weight_wait(p, b):
        remote(place(p, b), place(p, b), ws_sem.at[0, 0], wr_sem.at[p, b], mate_y).wait_recv()

    keep = [pltpu.make_async_copy(source(p, zz), place(p, sp), wl_sem.at[p]) for p in range(3)]
    other = [
        remote(source(p, 1 - zz), place(p, sp), ws_sem.at[0, p], wr_sem.at[p, sp], at(z + dz, y)) for p in range(3)
    ]
    same = [
        remote(source(p, zz), place(p, sp), ws_sem.at[1, p], wr_sem.at[p, sp], at(z + 2 * dz, y)) for p in range(3)
    ]
    outer_z = jnp.clip(z - dz, 0, 3)
    back = [
        remote(source(p, 1 - zz), place(p, sp), ws_sem.at[2, p], wr_sem.at[p, sp], at(outer_z, y)) for p in range(3)
    ]
    near = (2 * pair + 1 - zz) * 2 + y
    relay = [
        remote(place(p, near), place(p, near), ws_sem.at[3, p], wr_sem.at[p, near], at(z + 2 * dz, y))
        for p in range(3)
    ]
    across = [
        remote(source(p, zz), place(p, sp), wy_sem.at[0, p], wr_sem.at[p, sp], mate_y) for p in range(3)
    ]
    line = [near, (2 - pair) * 2 + y, (3 - 3 * pair) * 2 + y]
    spread = [
        [
            remote(place(p, b), place(p, b), wy_sem.at[1 + j, p], wr_sem.at[p, b], mate_y)
            for p in range(3)
        ]
        for j, b in enumerate(line)
    ]

    def first_sends(p):
        other[p].start()

        @pl.when(inner)
        def _():
            back[p].start()

        across[p].start()

    def service(j, p):
        weight_wait(p, line[j])
        spread[j][p].start()
        if j == 0:

            @pl.when(inner)
            def _():
                relay[p].start()

    first_sends(0)
    for copy in keep:
        copy.start()

    hrow[...] = jnp.zeros_like(hrow)
    srow[...] = jnp.zeros_like(srow)
    raw_s = steps_s[...].astype(F32)
    raw_l = steps_l[...].astype(F32)
    srow[0:heads1, :] = jnp.maximum(raw_s, 0.0) + jnp.log1p(jnp.exp(-jnp.abs(raw_s)))
    srow[heads1 : heads1 + heads2, :] = jnp.maximum(raw_l, 0.0) + jnp.log1p(jnp.exp(-jnp.abs(raw_l)))
    for h in range(heads1 + heads2):
        rate = rates_s[h] if h < heads1 else rates_l[h - heads1]
        offset = offs_s[h : h + 1, :] if h < heads1 else offs_l[h - heads1 : h - heads1 + 1, :]
        hrow[h : h + 1, :] = offset - jnp.exp(jnp.full((1, length), rate, F32)) * srow[h : h + 1, :]
    chunks = length // LANE
    ri = lax.broadcasted_iota(jnp.int32, (LANE, LANE), 0)
    ci = lax.broadcasted_iota(jnp.int32, (LANE, LANE), 1)
    upper = jnp.where(ri <= ci, 1.0, 0.0).astype(F32)
    slab = hrow.shape[0]
    stacked = jnp.concatenate([hrow[:, k * LANE : (k + 1) * LANE] for k in range(chunks)], axis=0)
    sums = lax.dot_general(
        stacked, upper, (((1,), (0,)), ((), ())), precision=HIGH, preferred_element_type=F32
    )
    base = jnp.zeros((slab, 1), F32)
    fill = jnp.zeros((LANE - 2 * slab, LANE), F32)
    for k in range(chunks):
        w = sums[k * slab : (k + 1) * slab] + base
        base = w[:, LANE - 1 : LANE]
        cut = slice(k * LANE, (k + 1) * LANE)
        wrow[:, cut] = w
        wcol[cut, :] = jnp.concatenate([w, srow[:, cut], fill], axis=0).T

    for copy in loads[:3]:
        copy.wait()

    @pl.when(sp > 0)
    def _():
        for copy in halos:
            copy.wait_recv()

    @pl.when(sp == 0)
    def _():
        xbuf[0:halo, :] = jnp.zeros((halo, width + planes), BF)

    def conv(lo, taps):
        wide = xbuf[:, lo : lo + LANE].astype(F32)
        total = wide * taps[-1]
        for k in range(len(taps) - 1):
            total = total + taps[k] * pltpu.roll(wide, len(taps) - 1 - k, 0)
        total = total[halo:]
        return total * jax.nn.sigmoid(total)

    count = taps_s.shape[0]
    for i in range(4):
        taps = [taps_m[k, i : i + 1, :].astype(F32) for k in range(count)]
        maps[:, i * LANE : (i + 1) * LANE] = conv(width + i * LANE, taps).astype(BF)
    lane = lax.broadcasted_iota(jnp.int32, (1, LANE), 1)
    size1, size2 = w1 // heads1, w2 // heads2

    def tile_heads(j):
        if j * LANE < w1:
            return [j * LANE // size1 + i for i in range(LANE // size1)], size1
        return [heads1 + (j * LANE - w1) // size2], size2

    def by_head(values, size):
        total = values[-1]
        for i in reversed(range(len(values) - 1)):
            total = jnp.where(lane < (i + 1) * size, values[i], total)
        return total

    def spread_cols(j, offset):
        own_heads, size = tile_heads(j)
        return by_head(
            [jnp.broadcast_to(wcol[:, offset + h : offset + h + 1], (length, LANE)) for h in own_heads], size
        )

    tiles = width // LANE
    slot = 0
    slots = {}
    for j in range(tiles):
        lo = j * LANE
        ref, at_lo = (taps_s, lo) if lo < w1 else (taps_l, lo - w1)
        taps = [ref[k : k + 1, at_lo : at_lo + LANE].astype(F32) for k in range(count)]
        driven = conv(lo, taps) * spread_cols(j, slab)
        own_heads, size = tile_heads(j)
        last = by_head([jnp.broadcast_to(wrow[h : h + 1, length - 1 : length], (1, LANE)) for h in own_heads], size)
        within = spread_cols(j, 0)
        late[:, lo : lo + LANE] = (driven * jnp.exp(last - within)).astype(BF)
        run[state : state + 1, lo : lo + LANE] = jnp.exp(last)
        for i, h in enumerate(own_heads):
            keep_lanes = driven
            if len(own_heads) > 1:
                keep_lanes = jnp.where((lane >= i * size) & (lane < (i + 1) * size), driven, 0.0)
            drv[:, slot * LANE : (slot + 1) * LANE] = keep_lanes.astype(BF)
            slots[h] = slot
            slot += 1

    for kind, lo, size in ((0, 0, w1), (1, w1, w2)):
        keys = maps[:, 2 * kind * LANE : (2 * kind + 1) * LANE]
        run[0:state, lo : lo + size] = lax.dot_general(
            keys, late[:, lo : lo + size], (((0,), (0,)), ((), ())), preferred_element_type=F32
        )
    run[state + 8 : 2 * state + 8, :] = jnp.zeros((state, width), F32)
    run[2 * state + 8 : 2 * state + 9, :] = jnp.ones((1, width), F32)
    messages = []
    while (1 << len(messages)) < n:
        k = len(messages)
        messages.append(
            remote(smsg.at[k], rmsg.at[k], ms_sem.at[k], mr_sem.at[k], (lax.rem(sp + (1 << k), n), tp))
        )

    def send_state(k):
        smsg[k, 0:state, :] = run[0:state, :].astype(BF)
        smsg[k, state : state + 16, :] = jnp.broadcast_to(run[state : state + 1, :], (16, width)).astype(BF)

        @pl.when(sp + (1 << k) < n)
        def _():
            messages[k].start()

    def take_state(k):
        @pl.when(sp >= (1 << k))
        def _():
            messages[k].wait_recv()
            got = rmsg[k, 0:state, :].astype(F32)
            decay = rmsg[k, state : state + 1, :].astype(F32)
            a, b = state + 8, 2 * state + 8
            before = run[b : b + 1, :]
            run[a:b, :] = got * before + run[a:b, :]
            run[b : b + 1, :] = decay * before
            if k + 1 < len(messages):
                here = run[state : state + 1, :]
                run[0:state, :] = got * here + run[0:state, :]
                run[state : state + 1, :] = decay * here

    kinds = [[h for h in slots if h < heads1], [h for h in slots if h >= heads1]]

    def local_rows(i):
        r0 = i * LANE
        size_k = r0 + LANE
        rowid = lax.broadcasted_iota(jnp.int32, (LANE, size_k), 0) + r0
        colid = lax.broadcasted_iota(jnp.int32, (LANE, size_k), 1)
        mask = colid <= rowid
        for kind in range(2):
            keys = maps[0:size_k, 2 * kind * LANE : (2 * kind + 1) * LANE]
            reads = maps[r0 : r0 + LANE, (2 * kind + 1) * LANE : (2 * kind + 2) * LANE]
            scores = lax.dot_general(reads, keys, (((1,), (1,)), ((), ())), preferred_element_type=F32)
            for j in range(tiles):
                own_heads, _ = tile_heads(j)
                if own_heads[0] not in kinds[kind]:
                    continue
                total = None
                for h in own_heads:
                    spread_h = wcol[r0 : r0 + LANE, h : h + 1] - wrow[h : h + 1, 0:size_k]
                    mixing = (jnp.exp(jnp.where(mask, spread_h, -1e30)) * scores).astype(BF)
                    term = jnp.dot(
                        mixing,
                        drv[0:size_k, slots[h] * LANE : (slots[h] + 1) * LANE],
                        preferred_element_type=F32,
                    )
                    total = term if total is None else total + term
                loc[r0 : r0 + LANE, j * LANE : (j + 1) * LANE] = total

    send_state(0)
    first_sends(1)
    cuts = [chunks * k // len(messages) for k in range(len(messages) + 1)]
    for k in range(len(messages)):
        for i in range(cuts[k], cuts[k + 1]):
            local_rows(i)
        take_state(k)
        if k + 1 < len(messages):
            send_state(k + 1)
        if k == 0:
            first_sends(2)
        if k == 1:
            for copy in same:
                copy.start()
            service(0, 0)
            service(0, 1)

    for copy in loads[3:]:
        copy.wait()
    for j in range(tiles):
        lo = j * LANE
        kind = 0 if lo < w1 else 1
        own_heads, size = tile_heads(j)
        reads = maps[:, (2 * kind + 1) * LANE : (2 * kind + 2) * LANE]
        carry = run[state + 8 : 2 * state + 8, lo : lo + LANE].astype(BF)
        carried = jnp.dot(reads, carry, preferred_element_type=F32)
        scan_out = loc[:, lo : lo + LANE] + carried * jnp.exp(spread_cols(j, 0))
        gates = gbuf[:, lo : lo + LANE].astype(F32)
        gated = scan_out * (gates * jax.nn.sigmoid(gates))
        square = gated * gated
        scales = []
        for i in range(len(own_heads)):
            one = square
            if len(own_heads) > 1:
                one = jnp.where((lane >= i * size) & (lane < (i + 1) * size), square, 0.0)
            mean = jnp.sum(one, axis=1, keepdims=True) * (1.0 / size)
            scales.append(jnp.broadcast_to(lax.rsqrt(mean + head_eps), (length, LANE)))
        ref, at_lo = (gain_s, lo) if lo < w1 else (gain_l, lo - w1)
        gain = ref[0:1, at_lo : at_lo + LANE]
        hbuf[:, lo : lo + LANE] = (gated * by_head(scales, size) * gain).astype(BF)

    wide = 2 * LANE

    @pl.loop(0, model // wide)
    def _(i):
        cut = pl.ds(pl.multiple_of(i * wide, wide), wide)
        part[:, cut] = jnp.dot(hbuf[...], pbuf[:, cut], preferred_element_type=F32).astype(BF)

    def rows_of(xi, ci):
        return pl.ds(pl.multiple_of((xi * 2 + ci) * own, own), own)

    cores = [
        remote(part.at[rows_of(xi, 1 - c), :], d2d.at[i], ds_sem.at[i], dr_sem.at[i], mate_c)
        for i, xi in enumerate((1 - x, x))
    ]
    for copy in cores:
        copy.start()
    service(0, 2)
    cores[0].wait_recv()
    xsend[...] = (part[rows_of(1 - x, c), :].astype(F32) + d2d[0].astype(F32)).astype(BF)
    cross = remote(xsend, xrecv, xs_sem.at[0], xr_sem.at[0], mate_x)
    cross.start()
    for p in range(3):
        service(1, p)
    cores[1].wait_recv()
    cross.wait_recv()
    mixed = part[rows_of(x, c), :].astype(F32) + d2d[1].astype(F32) + xrecv[...].astype(F32)
    middle = (rbuf[...].astype(F32) + mixed).astype(BF)
    mid[...] = middle
    broad = middle.astype(F32)
    scale = lax.rsqrt(jnp.mean(broad * broad, axis=-1, keepdims=True) + row_eps)

    def place_rows(zi, xi, ci):
        index = zi * 4 + ci * 2 + xi
        return index, nall.at[pl.ds(pl.multiple_of(index * own, own), own), :]

    _, my_rows = place_rows(zz, x, c)
    my_rows[...] = (broad * scale * cgain[...]).astype(BF)

    def share(i, zi, xi, ci, device):
        index, view = place_rows(zi, xi, ci)
        return remote(view, view, as_sem.at[i], ar_sem.at[index], device)

    def rows_wait(zi, xi, ci):
        share(0, zi, xi, ci, mate_c).wait_recv()

    shares = [
        share(0, zz, x, c, mate_x),
        share(1, zz, x, c, mate_z),
        share(2, zz, x, c, mate_c),
        share(3, zz, 1 - x, c, mate_c),
        share(4, 1 - zz, x, c, mate_x),
        share(5, 1 - zz, x, c, mate_c),
        share(6, 1 - zz, 1 - x, c, mate_c),
    ]
    for i in range(3):
        shares[i].start()
    rows_wait(zz, 1 - x, c)
    shares[3].start()
    rows_wait(1 - zz, x, c)
    shares[4].start()
    shares[5].start()

    for copy in keep:
        copy.wait()
    for p in range(2):
        service(2, p)

    far = [k * 2 + 1 - y for k in range(4)]
    for p in range(2):
        for b in far:
            weight_wait(p, b)
    rows_wait(zz, x, 1 - c)
    rows_wait(zz, 1 - x, 1 - c)
    hot = wide if half % wide == 0 else LANE
    first = zz * (2 * half - units)

    def up_rows(zi):
        span = pl.ds(pl.multiple_of(zi * (tokens // 2), tokens // 2), tokens // 2)

        @pl.loop(0, half // hot)
        def _(i):
            cut = pl.ds(pl.multiple_of(i * hot, hot), hot)
            have = nall[span, :]
            gate = jnp.dot(have, wg[:, cut], preferred_element_type=F32)
            up = jnp.dot(have, wu[:, cut], preferred_element_type=F32)
            unit = lax.broadcasted_iota(jnp.int32, (1, hot), 1) + i * hot
            value = gate * jax.nn.sigmoid(gate) * up
            hid[span, cut] = jnp.where(unit >= first, value, 0.0).astype(BF)

    up_rows(zz)
    rows_wait(1 - zz, 1 - x, c)
    shares[6].start()
    rows_wait(1 - zz, x, 1 - c)
    rows_wait(1 - zz, 1 - x, 1 - c)
    up_rows(1 - zz)
    service(2, 2)

    order = [
        ((2 * jnp.bitwise_xor(pair, dp) + k) * 2 + jnp.bitwise_xor(y, dy)) for dp in (0, 1) for dy in (0, 1) for k in (0, 1)
    ]
    known = [dy == 0 for _ in range(2) for dy in (0, 1) for _ in range(2)]
    core_rows = tokens // 4

    def strip(zi, ci):
        return pl.ds(pl.multiple_of(zi * (tokens // 2) + ci * core_rows, core_rows), core_rows)

    def swap(q):
        return [
            remote(
                psum.at[q, strip(zi, 1 - c), :],
                dcol.at[q, pl.ds(zi * core_rows, core_rows), :],
                p_sem.at[q, zi],
                q_sem.at[q, zi],
                mate_c,
            )
            for zi in range(2)
        ]

    def hop1(q):
        return remote(s1.at[q], r1.at[q], f1s_sem.at[q], f1r_sem.at[q], mate_z if q % 2 == 0 else mate_x)

    def hop2(q):
        return remote(s2.at[q], r2.at[q], f2s_sem.at[q], f2r_sem.at[q], mate_x if q % 2 == 0 else mate_z)

    def compute(q):
        if not known[q]:
            weight_wait(2, order[q])

        @pl.loop(0, 4)
        def _(i):
            span = pl.ds(pl.multiple_of(i * core_rows, core_rows), core_rows)
            psum[q, span, :] = jnp.dot(
                hid[span, :], wd[order[q]], preferred_element_type=F32
            ).astype(BF)

        for copy in swap(q):
            copy.start()

    def sum1(q):
        for copy in swap(q):
            copy.wait_recv()
        for j in range(2):
            for send in (True, False):
                if q % 2 == 0:
                    zi, xi = (1 - zz if send else zz), j
                else:
                    zi, xi = j, (1 - x if send else x)
                a = pl.ds(pl.multiple_of(zi * (tokens // 2) + c * core_rows + xi * own, own), own)
                b = pl.ds(pl.multiple_of(zi * core_rows + xi * own, own), own)
                total = psum[q, a, :].astype(F32) + dcol[q, b, :].astype(F32)
                to = slice(j * own, (j + 1) * own)
                if send:
                    s1[q, to, :] = total.astype(BF)
                else:
                    k1[q, to, :] = total
        hop1(q).start()

    def sum2(q):
        hop1(q).wait_recv()
        second = x if q % 2 == 0 else zz
        for send in (True, False):
            j = 1 - second if send else second
            cut = pl.ds(pl.multiple_of(j * own, own), own)
            total = k1[q, cut, :] + r1[q, cut, :].astype(F32)
            if send:
                s2[q] = total.astype(BF)
            else:
                k2[q] = total
        hop2(q).start()

    def sum3(q):
        hop2(q).wait_recv()
        cut = pl.ds(pl.multiple_of(order[q] * cols, cols), cols)
        out[:, cut] = (mid[:, cut].astype(F32) + k2[q] + r2[q].astype(F32)).astype(BF)

    stages = (compute, sum1, sum2, sum3)
    for step in range(n + len(stages) - 1):
        for i, stage in enumerate(stages):
            if 0 <= step - i < n:
                stage(step - i)

    @pl.when(sp < n - 1)
    def _():
        for copy in halos:
            copy.wait_send()

    for k, copy in enumerate(messages):

        @pl.when(sp + (1 << k) < n)
        def _(copy=copy):
            copy.wait_send()

    for p in range(3):
        other[p].wait_send()
        same[p].wait_send()
        across[p].wait_send()
        for j in range(3):
            spread[j][p].wait_send()

        @pl.when(inner)
        def _(p=p):
            back[p].wait_send()
            relay[p].wait_send()

    for copy in cores + [cross] + shares:
        copy.wait_send()
    for q in range(n):
        for copy in swap(q) + [hop1(q), hop2(q)]:
            copy.wait_send()


def fused_layer(
    residual,
    small_value_inputs,
    large_value_inputs,
    small_gate_inputs,
    large_gate_inputs,
    state_projections,
    small_step_inputs,
    large_step_inputs,
    small_decay_offsets,
    large_decay_offsets,
    small_decay_rates,
    large_decay_rates,
    small_filter_taps,
    large_filter_taps,
    state_filter_taps,
    small_head_gains,
    large_head_gains,
    small_output_projection,
    large_output_projection,
    channel_norm_gain,
    gate_matrix,
    up_matrix,
    down_matrix,
):
    n = lax.axis_size("sp")
    length, w1 = small_value_inputs.shape
    w2 = large_value_inputs.shape[1]
    width = w1 + w2
    state = state_projections.shape[2]
    planes = state_projections.shape[1] * state
    heads = small_decay_rates.shape[0] + large_decay_rates.shape[0]
    rows, units = gate_matrix.shape
    cols = down_matrix.shape[1]
    own, model = residual.shape
    tiles = units // LANE
    half = (tiles + 1) // 2 * LANE
    halo = 16
    slab = 8 * ((heads + 7) // 8)
    tokens = 2 * length
    hops = max(1, (n - 1).bit_length())
    vmem, dma = pltpu.VMEM, pltpu.SemaphoreType.DMA
    hbm = pl.BlockSpec(memory_space=pl.ANY)
    near = pl.BlockSpec(memory_space=pltpu.VMEM)
    scalar = pl.BlockSpec(memory_space=pltpu.SMEM)
    specs = [hbm] * 5 + [near] * 4 + [scalar] * 2 + [near] * 5 + [hbm] * 3 + [near] + [hbm] * 3
    scratch = [
        vmem((length + halo, width + planes), BF),
        vmem((length, width), BF),
        vmem((width, model), BF),
        vmem((own, model), BF),
        vmem((slab, length), F32),
        vmem((slab, length), F32),
        vmem((slab, length), F32),
        vmem((length, LANE), F32),
        vmem((length, planes), BF),
        vmem((length, heads * LANE), BF),
        vmem((length, width), BF),
        vmem((2 * state + 16, width), F32),
        vmem((hops, state + 16, width), BF),
        vmem((hops, state + 16, width), BF),
        vmem((length, width), F32),
        vmem((length, width), BF),
        vmem((length, model), BF),
        vmem((2, own, model), BF),
        vmem((own, model), BF),
        vmem((own, model), BF),
        vmem((own, model), BF),
        vmem((tokens, model), BF),
        vmem((tokens, half), BF),
        vmem((n * rows, half), BF),
        vmem((n * rows, half), BF),
        vmem((n, half, cols), BF),
        vmem((n, tokens, cols), BF),
        vmem((n, tokens // 2, cols), BF),
        vmem((n, 2 * own, cols), BF),
        vmem((n, 2 * own, cols), F32),
        vmem((n, 2 * own, cols), BF),
        vmem((n, own, cols), BF),
        vmem((n, own, cols), F32),
        vmem((n, own, cols), BF),
        dma((8,)),
        dma((3,)),
        dma((3,)),
        dma((4, 3)),
        dma((4, 3)),
        dma((3, n)),
        dma((3,)),
        dma((hops,)),
        dma((hops,)),
        dma((2,)),
        dma((2,)),
        dma((1,)),
        dma((1,)),
        dma((7,)),
        dma((8,)),
        dma((n, 2)),
        dma((n, 2)),
        dma((n,)),
        dma((n,)),
        dma((n,)),
        dma((n,)),
    ]
    return pl.pallas_call(
        fused_kernel,
        out_shape=jax.ShapeDtypeStruct((own, model), BF),
        in_specs=specs,
        out_specs=pl.BlockSpec(memory_space=pltpu.VMEM),
        scratch_shapes=scratch,
        compiler_params=pltpu.CompilerParams(
            collective_id=0, has_side_effects=True, vmem_limit_bytes=66 * 1024 * 1000
        ),
    )(
        small_value_inputs,
        large_value_inputs,
        small_gate_inputs,
        large_gate_inputs,
        state_projections.reshape(length, planes),
        small_step_inputs.T,
        large_step_inputs.T,
        small_decay_offsets.T,
        large_decay_offsets.T,
        small_decay_rates,
        large_decay_rates,
        small_filter_taps,
        large_filter_taps,
        state_filter_taps,
        small_head_gains.reshape(1, w1),
        large_head_gains.reshape(1, w2),
        small_output_projection,
        large_output_projection,
        residual,
        channel_norm_gain.reshape(1, model),
        gate_matrix,
        up_matrix,
        down_matrix,
    )


def solution(mesh):
    in_specs = (
        P(("sp", "tp"), None),
        P("sp", "tp"),
        P("sp", "tp"),
        P("sp", "tp"),
        P("sp", "tp"),
        P("sp", None, None),
        P("sp", "tp"),
        P("sp", "tp"),
        P("sp", "tp"),
        P("sp", "tp"),
        P("tp"),
        P("tp"),
        P(None, "tp"),
        P(None, "tp"),
        P(),
        P("tp"),
        P("tp"),
        P("tp", None),
        P("tp", None),
        P(),
        P("sp", "tp"),
        P("sp", "tp"),
        P("tp", "sp"),
    )

    def layer(*args):
        units = args[20].shape[1]
        if paired(mesh.shape["sp"], mesh.shape["tp"], units):
            return fused_layer(*args)
        return on_device(*args)

    return jax.shard_map(
        layer,
        mesh=mesh,
        in_specs=in_specs,
        out_specs=P(("sp", "tp"), None),
        check_vma=False,
    )
```

profile of v0, /device:TPU:16, one launch (start us, length us, event | category | flops | bytes accessed | tf_op | source)
XLA Modules:
  0.0 203.9 jit_solution(6118388082877994534)
XLA Ops:
  0.0 2.0 copy.26
  2.0 199.9 %shard_map.217 = bf16[160,2048]{1,0:T(8,128)(2,1)} custom-call(bf16[640,256]{1,0:T(8,128)(2,1)} %vs.1, bf16[640,256]{1,0:T(8,128)(2,1)} %vl.1, bf16[640,256]{1,0:T(8,128)(2,1)} %gs.1, bf16[640,256]{1,0:T(8,128)(2,1)} %gl.1, bf16[640,512]{1,0:T(8,128)(2,1)} %bitcast.11, bf16[4,640]{1,0:T(4,128)(2,1)} %bitcast.15, bf16[2,640]{1,0:T(2,128)(2,1)} %bitcast.17, ...), custom_call_target="tpu_custom_call" | custom-call | tf_op jit(solution)/shard_map/pallas_call | solution.py:961
  201.9 2.0 copy.28
where the time goes:
time: 204 us
  Pallas kernels  200 us (98%)
  local copies, waits for them, and re-layouts  4.01 us (2%)
    pallas_call x1, Pallas kernels, fused_layer(): pl.pallas_call(fused_kernel, out_shape=jax.ShapeDtypeStruct((own, model),...  200 us

commit v1 on v0

--- a/solution.py
+++ b/solution.py
@@ -423,14 +423,12 @@
         for j, b in enumerate(line)
     ]
 
-    def first_sends(p):
+    def start_line(p):
         other[p].start()
 
         @pl.when(inner)
         def _():
             back[p].start()
-
-        across[p].start()
 
     def service(j, p):
         weight_wait(p, line[j])
@@ -441,7 +439,7 @@
             def _():
                 relay[p].start()
 
-    first_sends(0)
+    start_line(0)
     for copy in keep:
         copy.start()
 
@@ -543,37 +541,74 @@
         run[0:state, lo : lo + size] = lax.dot_general(
             keys, late[:, lo : lo + size], (((0,), (0,)), ((), ())), preferred_element_type=F32
         )
-    run[state + 8 : 2 * state + 8, :] = jnp.zeros((state, width), F32)
-    run[2 * state + 8 : 2 * state + 9, :] = jnp.ones((1, width), F32)
-    messages = []
-    while (1 << len(messages)) < n:
-        k = len(messages)
-        messages.append(
-            remote(smsg.at[k], rmsg.at[k], ms_sem.at[k], mr_sem.at[k], (lax.rem(sp + (1 << k), n), tp))
-        )
-
-    def send_state(k):
+    lo_y, hi_y = state + 8, 2 * state + 8
+    run[lo_y:hi_y, :] = jnp.zeros((state, width), F32)
+    run[hi_y : hi_y + 1, :] = jnp.ones((1, width), F32)
+    ahead = at(jnp.minimum(z + 1, 3), y)
+    ahead2 = at(jnp.minimum(z + 2, 3), y)
+    messages = [
+        remote(smsg.at[0], rmsg.at[0], ms_sem.at[0], mr_sem.at[0], mate_y),
+        remote(smsg.at[1], rmsg.at[1], ms_sem.at[1], mr_sem.at[1], ahead),
+        remote(smsg.at[2], rmsg.at[2], ms_sem.at[2], mr_sem.at[2], ahead),
+        remote(smsg.at[2], rmsg.at[2], ms_sem.at[3], mr_sem.at[2], ahead2),
+    ]
+    bridge = z == 1
+
+    def write_state(k):
         smsg[k, 0:state, :] = run[0:state, :].astype(BF)
         smsg[k, state : state + 16, :] = jnp.broadcast_to(run[state : state + 1, :], (16, width)).astype(BF)
 
-        @pl.when(sp + (1 << k) < n)
+    def got_state(k):
+        return rmsg[k, 0:state, :].astype(F32), rmsg[k, state : state + 1, :].astype(F32)
+
+    def extend(got, decay):
+        before = run[hi_y : hi_y + 1, :]
+        run[lo_y:hi_y, :] = got * before + run[lo_y:hi_y, :]
+        run[hi_y : hi_y + 1, :] = decay * before
+
+    def put_before(got, decay):
+        here = run[state : state + 1, :]
+        run[0:state, :] = got * here + run[0:state, :]
+        run[state : state + 1, :] = decay * here
+
+    def take_row():
+        messages[0].wait_recv()
+        got, decay = got_state(0)
+
+        @pl.when(y == 1)
         def _():
-            messages[k].start()
-
-    def take_state(k):
-        @pl.when(sp >= (1 << k))
+            extend(got, decay)
+            put_before(got, decay)
+
+        @pl.when(y == 0)
         def _():
-            messages[k].wait_recv()
-            got = rmsg[k, 0:state, :].astype(F32)
-            decay = rmsg[k, state : state + 1, :].astype(F32)
-            a, b = state + 8, 2 * state + 8
-            before = run[b : b + 1, :]
-            run[a:b, :] = got * before + run[a:b, :]
-            run[b : b + 1, :] = decay * before
-            if k + 1 < len(messages):
-                here = run[state : state + 1, :]
-                run[0:state, :] = got * here + run[0:state, :]
-                run[state : state + 1, :] = decay * here
+            run[0:state, :] = run[0:state, :] * decay + got
+            run[state : state + 1, :] = run[state : state + 1, :] * decay
+
+        @pl.when(zz == 0)
+        def _():
+            write_state(1)
+            messages[1].start()
+
+    def take_half():
+        @pl.when(zz == 1)
+        def _():
+            messages[1].wait_recv()
+            got, decay = got_state(1)
+            extend(got, decay)
+            put_before(got, decay)
+
+            @pl.when(bridge)
+            def _():
+                write_state(2)
+                messages[2].start()
+                messages[3].start()
+
+    def take_rest():
+        @pl.when(pair == 1)
+        def _():
+            messages[2].wait_recv()
+            extend(*got_state(2))
 
     kinds = [[h for h in slots if h < heads1], [h for h in slots if h >= heads1]]
 
@@ -603,22 +638,37 @@
                     total = term if total is None else total + term
                 loc[r0 : r0 + LANE, j * LANE : (j + 1) * LANE] = total
 
-    send_state(0)
-    first_sends(1)
-    cuts = [chunks * k // len(messages) for k in range(len(messages) + 1)]
-    for k in range(len(messages)):
-        for i in range(cuts[k], cuts[k + 1]):
-            local_rows(i)
-        take_state(k)
-        if k + 1 < len(messages):
-            send_state(k + 1)
-        if k == 0:
-            first_sends(2)
-        if k == 1:
-            for copy in same:
-                copy.start()
-            service(0, 0)
-            service(0, 1)
+    write_state(0)
+    messages[0].start()
+    across[0].start()
+    mark = (chunks + 1) // 2
+    for i in range(mark):
+        local_rows(i)
+    take_row()
+    start_line(1)
+    across[1].start()
+    for i in range(mark, chunks):
+        local_rows(i)
+    take_half()
+
+    @pl.when(inner)
+    def _():
+        same[0].start()
+        same[1].start()
+
+    @pl.when(jnp.logical_not(inner))
+    def _():
+        other[2].start()
+
+    service(0, 0)
+    service(0, 1)
+
+    @pl.when(jnp.logical_not(inner))
+    def _():
+        same[0].start()
+        same[1].start()
+
+    take_rest()
 
     for copy in loads[3:]:
         copy.wait()
@@ -660,13 +710,11 @@
     ]
     for copy in cores:
         copy.start()
-    service(0, 2)
     cores[0].wait_recv()
     xsend[...] = (part[rows_of(1 - x, c), :].astype(F32) + d2d[0].astype(F32)).astype(BF)
     cross = remote(xsend, xrecv, xs_sem.at[0], xr_sem.at[0], mate_x)
     cross.start()
-    for p in range(3):
-        service(1, p)
+    service(1, 0)
     cores[1].wait_recv()
     cross.wait_recv()
     mixed = part[rows_of(x, c), :].astype(F32) + d2d[1].astype(F32) + xrecv[...].astype(F32)
@@ -700,16 +748,34 @@
     ]
     for i in range(3):
         shares[i].start()
+
+    @pl.when(inner)
+    def _():
+        other[2].start()
+        back[2].start()
+
+    same[2].start()
+
+    @pl.when(inner)
+    def _():
+        weight_wait(2, near)
+        relay[2].start()
+        spread[0][2].start()
+
+    across[2].start()
+    service(1, 1)
     rows_wait(zz, 1 - x, c)
     shares[3].start()
+    for p in range(2):
+        service(2, p)
     rows_wait(1 - zz, x, c)
     shares[4].start()
     shares[5].start()
 
     for copy in keep:
         copy.wait()
-    for p in range(2):
-        service(2, p)
+
+    service(1, 2)
 
     far = [k * 2 + 1 - y for k in range(4)]
     for p in range(2):
@@ -739,12 +805,10 @@
     rows_wait(1 - zz, x, 1 - c)
     rows_wait(1 - zz, 1 - x, 1 - c)
     up_rows(1 - zz)
-    service(2, 2)
-
-    order = [
-        ((2 * jnp.bitwise_xor(pair, dp) + k) * 2 + jnp.bitwise_xor(y, dy)) for dp in (0, 1) for dy in (0, 1) for k in (0, 1)
-    ]
-    known = [dy == 0 for _ in range(2) for dy in (0, 1) for _ in range(2)]
+
+    order = [zi * 2 + yi for yi in (y, 1 - y) for zi in (3 * pair, 2 - pair, 1 + pair, 3 - 3 * pair)]
+    known = [True] * 4 + [False] * 4
+    z_first = [False] * (n - 2) + [True, False]
     core_rows = tokens // 4
 
     def strip(zi, ci):
@@ -763,12 +827,21 @@
         ]
 
     def hop1(q):
-        return remote(s1.at[q], r1.at[q], f1s_sem.at[q], f1r_sem.at[q], mate_z if q % 2 == 0 else mate_x)
+        return remote(s1.at[q], r1.at[q], f1s_sem.at[q], f1r_sem.at[q], mate_z if z_first[q] else mate_x)
 
     def hop2(q):
-        return remote(s2.at[q], r2.at[q], f2s_sem.at[q], f2r_sem.at[q], mate_x if q % 2 == 0 else mate_z)
+        return remote(s2.at[q], r2.at[q], f2s_sem.at[q], f2r_sem.at[q], mate_x if z_first[q] else mate_z)
 
     def compute(q):
+        if q == 2:
+
+            @pl.when(jnp.logical_not(inner))
+            def _():
+                weight_wait(2, near)
+                spread[0][2].start()
+
+        if q == 3:
+            service(2, 2)
         if not known[q]:
             weight_wait(2, order[q])
 
@@ -787,7 +860,7 @@
             copy.wait_recv()
         for j in range(2):
             for send in (True, False):
-                if q % 2 == 0:
+                if z_first[q]:
                     zi, xi = (1 - zz if send else zz), j
                 else:
                     zi, xi = j, (1 - x if send else x)
@@ -803,7 +876,7 @@
 
     def sum2(q):
         hop1(q).wait_recv()
-        second = x if q % 2 == 0 else zz
+        second = x if z_first[q] else zz
         for send in (True, False):
             j = 1 - second if send else second
             cut = pl.ds(pl.multiple_of(j * own, own), own)
@@ -830,11 +903,16 @@
         for copy in halos:
             copy.wait_send()
 
-    for k, copy in enumerate(messages):
-
-        @pl.when(sp + (1 << k) < n)
-        def _(copy=copy):
-            copy.wait_send()
+    messages[0].wait_send()
+
+    @pl.when(zz == 0)
+    def _():
+        messages[1].wait_send()
+
+    @pl.when(bridge)
+    def _():
+        messages[2].wait_send()
+        messages[3].wait_send()
 
     for p in range(3):
         other[p].wait_send()
@@ -895,7 +973,7 @@
     halo = 16
     slab = 8 * ((heads + 7) // 8)
     tokens = 2 * length
-    hops = max(1, (n - 1).bit_length())
+    hops = 3
     vmem, dma = pltpu.VMEM, pltpu.SemaphoreType.DMA
     hbm = pl.BlockSpec(memory_space=pl.ANY)
     near = pl.BlockSpec(memory_space=pltpu.VMEM)
@@ -943,8 +1021,8 @@
         dma((4, 3)),
         dma((3, n)),
         dma((3,)),
-        dma((hops,)),
-        dma((hops,)),
+        dma((4,)),
+        dma((3,)),
         dma((2,)),
         dma((2,)),
         dma((1,)),

time: 204 us -> 163 us (0.80)
  Pallas kernels: 200 us -> 159 us
    pallas_call x1, Pallas kernels: 200 us -> 159 us  [fused_layer(): pl.pallas_call(fused_kernel, out_shape=jax.ShapeDtypeStruct((own, model),...]
where the time goes in v1:
time: 163 us
  Pallas kernels  159 us (98%)
  local copies, waits for them, and re-layouts  4.01 us (2%)
    pallas_call x1, Pallas kernels, fused_layer(): pl.pallas_call(fused_kernel, out_shape=jax.ShapeDtypeStruct((own, model),...  159 us
    unnamed x2, local copies, waits for them, and re-layouts  4.01 us

profile of v1, /device:TPU:16, one launch (start us, length us, event | category | flops | bytes accessed | tf_op | source)
XLA Modules:
  0.0 163.0 jit_solution(399656027495097766)
XLA Ops:
  0.0 2.0 %copy.26 = bf16[80,8,4,128]{3,1,2,0:T(8,128)(2,1)} copy(bf16[80,8,4,128]{3,2,1,0:T(4,128)(2,1)} %bitcast.12) | data formatting | bytes 1310720
  2.0 159.0 %shard_map.217 = bf16[160,2048]{1,0:T(8,128)(2,1)} custom-call(bf16[640,256]{1,0:T(8,128)(2,1)} %vs.1, bf16[640,256]{1,0:T(8,128)(2,1)} %vl.1, bf16[640,256]{1,0:T(8,128)(2,1)} %gs.1, bf16[640,256]{1,0:T(8,128)(2,1)} %gl.1, bf16[640,512]{1,0:T(8,128)(2,1)} %bitcast.11, bf16[4,640]{1,0:T(4,128)(2,1)} %bitcast.15, bf16[2,640]{1,0:T(2,128)(2,1)} %bitcast.17, ...), custom_call_target="tpu_custom_call" | custom-call | tf_op jit(solution)/shard_map/pallas_call | solution.py:1039
  161.0 2.0 %copy.28 = bf16[160,2048]{1,0:T(8,128)(2,1)} copy(bf16[160,2048]{1,0:T(8,128)(2,1)} %shard_map.217) | data formatting | bytes 1310720

commit v2 on v1

--- a/solution.py
+++ b/solution.py
@@ -227,7 +227,7 @@
 
 def paired(n, tp, units):
     ys, zs = geometry(n)
-    return ys == 2 and zs == 4 and tp == 4 and units % LANE == 0
+    return ys == 2 and zs == 4 and tp == 4 and units % (2 * LANE) == LANE
 
 
 def fused_kernel(
@@ -281,6 +281,9 @@
     wg,
     wu,
     wd,
+    seams,
+    seam_gate,
+    seam_up,
     psum,
     dcol,
     s1,
@@ -326,7 +329,9 @@
     rows, units = gate_m.shape
     cols = down_m.shape[1]
     half = wg.shape[1]
-    lift = units - half
+    seam = LANE // 2
+    main = half - LANE
+    share_units = units // 2
     own = resid.shape[0]
     tokens = nall.shape[0]
     model = nall.shape[1]
@@ -364,6 +369,12 @@
         copy = pltpu.make_async_copy(src, dst, lsem.at[len(loads)])
         copy.start()
         loads.append(copy)
+    tiles5 = [
+        pltpu.make_async_copy(src.at[:, pl.ds(main, LANE)], dst, lsem.at[len(loads) + i])
+        for i, (src, dst) in enumerate(((gate_m, seam_gate), (up_m, seam_up)))
+    ]
+    for copy in tiles5:
+        copy.start()
     pl.semaphore_wait(barrier, len(peers))
 
     halos = []
@@ -383,65 +394,91 @@
         for copy in halos:
             copy.start()
 
+    def lanes(start, size):
+        return pl.ds(pl.multiple_of(start, LANE), size)
+
     def source(p, h):
-        cut = pl.ds(pl.multiple_of(h * lift, LANE), half)
-        return (gate_m.at[:, cut], up_m.at[:, cut], down_m.at[cut, :])[p]
-
-    def place(p, b):
         if p == 2:
-            return wd.at[b]
-        return (wg, wu)[p].at[pl.ds(pl.multiple_of(b * rows, rows), rows), :]
+            return down_m.at[pl.ds(pl.multiple_of(h * share_units, seam), share_units), :]
+        if p == 3:
+            return seams.at[h]
+        return (gate_m, up_m)[p].at[:, lanes(h * half, main)]
+
+    def place(p, b, h):
+        if p == 2:
+            return wd.at[b, pl.ds(pl.multiple_of(h * seam, seam), share_units), :]
+        block = pl.ds(pl.multiple_of(b * rows, rows), rows)
+        if p == 3:
+            return wg.at[block, lanes((1 - h) * main, LANE)]
+        return (wg, wu)[p].at[block, lanes(h * LANE, main)]
 
     def weight_wait(p, b):
-        remote(place(p, b), place(p, b), ws_sem.at[0, 0], wr_sem.at[p, b], mate_y).wait_recv()
-
-    keep = [pltpu.make_async_copy(source(p, zz), place(p, sp), wl_sem.at[p]) for p in range(3)]
-    other = [
-        remote(source(p, 1 - zz), place(p, sp), ws_sem.at[0, p], wr_sem.at[p, sp], at(z + dz, y)) for p in range(3)
-    ]
-    same = [
-        remote(source(p, zz), place(p, sp), ws_sem.at[1, p], wr_sem.at[p, sp], at(z + 2 * dz, y)) for p in range(3)
-    ]
-    outer_z = jnp.clip(z - dz, 0, 3)
-    back = [
-        remote(source(p, 1 - zz), place(p, sp), ws_sem.at[2, p], wr_sem.at[p, sp], at(outer_z, y)) for p in range(3)
-    ]
+        remote(place(p, b, zz), place(p, b, zz), ws_sem.at[0, 0], wr_sem.at[p, b], mate_y).wait_recv()
+
+    pieces = range(4)
+    groups = ((0,), (1, 3), (2,))
+    keep = [pltpu.make_async_copy(source(p, zz), place(p, sp, zz), wl_sem.at[p]) for p in pieces]
+
+    def own_sends(kind, h, device):
+        return [
+            remote(source(p, h), place(p, sp, h), ws_sem.at[kind, p], wr_sem.at[p, sp], device) for p in pieces
+        ]
+
+    other = own_sends(0, 1 - zz, at(z + dz, y))
+    same = own_sends(1, zz, at(z + 2 * dz, y))
+    back = own_sends(2, 1 - zz, at(jnp.clip(z - dz, 0, 3), y))
     near = (2 * pair + 1 - zz) * 2 + y
     relay = [
-        remote(place(p, near), place(p, near), ws_sem.at[3, p], wr_sem.at[p, near], at(z + 2 * dz, y))
-        for p in range(3)
+        remote(place(p, near, zz), place(p, near, zz), ws_sem.at[3, p], wr_sem.at[p, near], at(z + 2 * dz, y))
+        for p in pieces
     ]
     across = [
-        remote(source(p, zz), place(p, sp), wy_sem.at[0, p], wr_sem.at[p, sp], mate_y) for p in range(3)
+        remote(source(p, zz), place(p, sp, zz), wy_sem.at[0, p], wr_sem.at[p, sp], mate_y) for p in pieces
     ]
     line = [near, (2 - pair) * 2 + y, (3 - 3 * pair) * 2 + y]
     spread = [
         [
-            remote(place(p, b), place(p, b), wy_sem.at[1 + j, p], wr_sem.at[p, b], mate_y)
-            for p in range(3)
+            remote(place(p, b, zz), place(p, b, zz), wy_sem.at[1 + j, p], wr_sem.at[p, b], mate_y)
+            for p in pieces
         ]
         for j, b in enumerate(line)
     ]
 
-    def start_line(p):
-        other[p].start()
-
-        @pl.when(inner)
+    def start(copies, g):
+        for p in groups[g]:
+            copies[p].start()
+
+    def arrived(j, g):
+        for p in groups[g]:
+            weight_wait(p, line[j])
+
+    def service(j, g):
+        arrived(j, g)
+        start(spread[j], g)
+
+    def only(cond, *actions):
+        @pl.when(cond)
         def _():
-            back[p].start()
-
-    def service(j, p):
-        weight_wait(p, line[j])
-        spread[j][p].start()
-        if j == 0:
-
-            @pl.when(inner)
-            def _():
-                relay[p].start()
-
-    start_line(0)
-    for copy in keep:
-        copy.start()
+            for action, *args in actions:
+                action(*args)
+
+    outer = jnp.logical_not(inner)
+    z0, z1, z2, z3 = [z == k for k in range(4)]
+
+    only(inner, (start, same, 0), (start, other, 0), (start, back, 0))
+    only(outer, (start, other, 0))
+    for p in range(3):
+        keep[p].start()
+    for copy in tiles5:
+        copy.wait()
+    left = lax.broadcasted_iota(jnp.int32, (1, LANE), 1) < seam
+    turned = pltpu.roll(seam_up[...].astype(F32), seam, 1)
+    plain = seam_gate[...].astype(F32)
+    seams[0] = jnp.where(left, plain, turned).astype(BF)
+    seams[1] = jnp.where(left, turned, plain).astype(BF)
+    wu[:, lanes((1 - zz) * main, LANE)] = jnp.zeros((n * rows, LANE), BF)
+    for b in range(n):
+        wd[b, pl.ds(pl.multiple_of((1 - zz) * share_units, seam), seam), :] = jnp.zeros((seam, cols), BF)
 
     hrow[...] = jnp.zeros_like(hrow)
     srow[...] = jnp.zeros_like(srow)
@@ -640,34 +677,25 @@
 
     write_state(0)
     messages[0].start()
-    across[0].start()
+    keep[3].start()
+    start(across, 0)
+    start(across, 1)
+
+    only(z1, (start, back, 1))
+    only(z2, (service, 0, 0), (start, relay, 0), (start, same, 1), (start, other, 1))
+    only(z3, (start, other, 1))
     mark = (chunks + 1) // 2
     for i in range(mark):
         local_rows(i)
     take_row()
-    start_line(1)
-    across[1].start()
+    only(z0, (start, other, 1))
+    only(z2, (start, back, 1))
     for i in range(mark, chunks):
         local_rows(i)
     take_half()
-
-    @pl.when(inner)
-    def _():
-        same[0].start()
-        same[1].start()
-
-    @pl.when(jnp.logical_not(inner))
-    def _():
-        other[2].start()
-
-    service(0, 0)
-    service(0, 1)
-
-    @pl.when(jnp.logical_not(inner))
-    def _():
-        same[0].start()
-        same[1].start()
-
+    only(z1, (service, 0, 0), (start, relay, 0), (start, same, 1), (start, other, 1))
+    only(inner, (service, 0, 1), (start, relay, 1))
+    only(outer, (service, 0, 0), (start, other, 2))
     take_rest()
 
     for copy in loads[3:]:
@@ -710,11 +738,13 @@
     ]
     for copy in cores:
         copy.start()
+    only(outer, (start, same, 0), (start, same, 1), (start, across, 2))
     cores[0].wait_recv()
     xsend[...] = (part[rows_of(1 - x, c), :].astype(F32) + d2d[0].astype(F32)).astype(BF)
     cross = remote(xsend, xrecv, xs_sem.at[0], xr_sem.at[0], mate_x)
     cross.start()
     service(1, 0)
+    only(outer, (service, 2, 0))
     cores[1].wait_recv()
     cross.wait_recv()
     mixed = part[rows_of(x, c), :].astype(F32) + d2d[1].astype(F32) + xrecv[...].astype(F32)
@@ -749,42 +779,32 @@
     for i in range(3):
         shares[i].start()
 
-    @pl.when(inner)
-    def _():
-        other[2].start()
-        back[2].start()
-
-    same[2].start()
-
-    @pl.when(inner)
-    def _():
-        weight_wait(2, near)
-        relay[2].start()
-        spread[0][2].start()
-
-    across[2].start()
+    start(same, 2)
+    only(inner, (start, other, 2), (start, back, 2), (arrived, 0, 2), (start, relay, 2), (start, across, 2))
+    only(outer, (service, 0, 1))
+    only(z2, (service, 2, 0))
     service(1, 1)
+    only(outer, (service, 2, 1))
     rows_wait(zz, 1 - x, c)
     shares[3].start()
-    for p in range(2):
-        service(2, p)
+    only(z1, (service, 2, 0))
     rows_wait(1 - zz, x, c)
     shares[4].start()
     shares[5].start()
-
+    only(inner, (service, 2, 1), (start, spread[0], 2))
+
+    far = [k * 2 + 1 - y for k in range(4)]
     for copy in keep:
         copy.wait()
-
-    service(1, 2)
-
-    far = [k * 2 + 1 - y for k in range(4)]
-    for p in range(2):
+    for p in (0, 1, 3):
         for b in far:
             weight_wait(p, b)
     rows_wait(zz, x, 1 - c)
     rows_wait(zz, 1 - x, 1 - c)
     hot = wide if half % wide == 0 else LANE
-    first = zz * (2 * half - units)
+    first = zz * seam
+    shared = (1 - zz) * main
+    turn = seam + (1 - zz) * (hot - 2 * seam)
 
     def up_rows(zi):
         span = pl.ds(pl.multiple_of(zi * (tokens // 2), tokens // 2), tokens // 2)
@@ -796,10 +816,15 @@
             gate = jnp.dot(have, wg[:, cut], preferred_element_type=F32)
             up = jnp.dot(have, wu[:, cut], preferred_element_type=F32)
             unit = lax.broadcasted_iota(jnp.int32, (1, hot), 1) + i * hot
+            up = jnp.where((unit >= shared) & (unit < shared + LANE), pltpu.roll(gate, turn, 1), up)
             value = gate * jax.nn.sigmoid(gate) * up
-            hid[span, cut] = jnp.where(unit >= first, value, 0.0).astype(BF)
+            used = (unit >= first) & (unit < first + share_units)
+            hid[span, cut] = jnp.where(used, value, 0.0).astype(BF)
 
     up_rows(zz)
+
+    service(1, 2)
+    only(outer, (service, 0, 2))
     rows_wait(1 - zz, 1 - x, c)
     shares[6].start()
     rows_wait(1 - zz, x, 1 - c)
@@ -808,7 +833,7 @@
 
     order = [zi * 2 + yi for yi in (y, 1 - y) for zi in (3 * pair, 2 - pair, 1 + pair, 3 - 3 * pair)]
     known = [True] * 4 + [False] * 4
-    z_first = [False] * (n - 2) + [True, False]
+    z_first = [q % 2 == 1 for q in range(n)]
     core_rows = tokens // 4
 
     def strip(zi, ci):
@@ -833,13 +858,6 @@
         return remote(s2.at[q], r2.at[q], f2s_sem.at[q], f2r_sem.at[q], mate_x if z_first[q] else mate_z)
 
     def compute(q):
-        if q == 2:
-
-            @pl.when(jnp.logical_not(inner))
-            def _():
-                weight_wait(2, near)
-                spread[0][2].start()
-
         if q == 3:
             service(2, 2)
         if not known[q]:
@@ -892,11 +910,11 @@
         cut = pl.ds(pl.multiple_of(order[q] * cols, cols), cols)
         out[:, cut] = (mid[:, cut].astype(F32) + k2[q] + r2[q].astype(F32)).astype(BF)
 
-    stages = (compute, sum1, sum2, sum3)
-    for step in range(n + len(stages) - 1):
-        for i, stage in enumerate(stages):
-            if 0 <= step - i < n:
-                stage(step - i)
+    stages = ((sum1, 2), (sum2, 4), (compute, 0), (sum3, 6))
+    for step in range(n + 6):
+        for stage, lag in stages:
+            if 0 <= step - lag < n:
+                stage(step - lag)
 
     @pl.when(sp < n - 1)
     def _():
@@ -914,7 +932,7 @@
         messages[2].wait_send()
         messages[3].wait_send()
 
-    for p in range(3):
+    for p in pieces:
         other[p].wait_send()
         same[p].wait_send()
         across[p].wait_send()
@@ -1006,6 +1024,9 @@
         vmem((n * rows, half), BF),
         vmem((n * rows, half), BF),
         vmem((n, half, cols), BF),
+        vmem((2, rows, LANE), BF),
+        vmem((rows, LANE), BF),
+        vmem((rows, LANE), BF),
         vmem((n, tokens, cols), BF),
         vmem((n, tokens // 2, cols), BF),
         vmem((n, 2 * own, cols), BF),
@@ -1014,13 +1035,13 @@
         vmem((n, own, cols), BF),
         vmem((n, own, cols), F32),
         vmem((n, own, cols), BF),
-        dma((8,)),
+        dma((10,)),
         dma((3,)),
         dma((3,)),
-        dma((4, 3)),
-        dma((4, 3)),
-        dma((3, n)),
-        dma((3,)),
+        dma((4, 4)),
+        dma((4, 4)),
+        dma((4, n)),
+        dma((4,)),
         dma((4,)),
         dma((3,)),
         dma((2,)),

time: 163 us -> 144 us (0.88)
  Pallas kernels: 159 us -> 139 us
    pallas_call x1, Pallas kernels: 159 us -> 139 us  [fused_layer(): pl.pallas_call(fused_kernel, out_shape=jax.ShapeDtypeStruct((own, model),...]
where the time goes in v2:
time: 144 us; the launch traced here: 143 us
  Pallas kernels  139 us (97%)
  local copies, waits for them, and re-layouts  4.01 us (3%)
    pallas_call x1, Pallas kernels, fused_layer(): pl.pallas_call(fused_kernel, out_shape=jax.ShapeDtypeStruct((own, model),...  139 us
    unnamed x2, local copies, waits for them, and re-layouts  4.01 us

profile of v2, /device:TPU:16, one launch (start us, length us, event | category | flops | bytes accessed | tf_op | source)
XLA Modules:
  0.0 142.6 jit_solution(2949789544673991535)
XLA Ops:
  0.0 2.0 %copy.26 = bf16[80,8,4,128]{3,1,2,0:T(8,128)(2,1)} copy(bf16[80,8,4,128]{3,2,1,0:T(4,128)(2,1)} %bitcast.12) | data formatting | bytes 1310720
  2.0 138.6 %shard_map.217 = bf16[160,2048]{1,0:T(8,128)(2,1)} custom-call(bf16[640,256]{1,0:T(8,128)(2,1)} %vs.1, bf16[640,256]{1,0:T(8,128)(2,1)} %vl.1, bf16[640,256]{1,0:T(8,128)(2,1)} %gs.1, bf16[640,256]{1,0:T(8,128)(2,1)} %gl.1, bf16[640,512]{1,0:T(8,128)(2,1)} %bitcast.11, bf16[4,640]{1,0:T(4,128)(2,1)} %bitcast.15, bf16[2,640]{1,0:T(2,128)(2,1)} %bitcast.17, ...), custom_call_target="tpu_custom_call" | custom-call | tf_op jit(solution)/shard_map/pallas_call | solution.py:1060
  140.6 2.0 %copy.28 = bf16[160,2048]{1,0:T(8,128)(2,1)} copy(bf16[160,2048]{1,0:T(8,128)(2,1)} %shard_map.217) | data formatting | bytes 1310720
